TPU v7x, 32 devices: a whole 2x2x4 slice. The times are simulated.
32 devices in a mesh: grp: 2 (over y), sp: 4 (over z), tp: 4 (over x, core).
Axes of the slice: x: 2, y: 2, z: 4, core: 2. Of those that a mesh axis runs over, the one named last changes fastest.
Arguments:
- hidden_in: bfloat16 [3072, 4096], P(('grp', 'sp'), 'tp'), parts along dimension 0, may hold values from -30 to 30
- in_gain: float32 [2, 4096], P(None, 'tp'), may hold values from 0.1 to 1.9
- w_value: bfloat16 [2, 4096, 2048], P(None, 'sp', 'tp'), may hold values from -0.09375 to 0.09375
- w_gate: bfloat16 [2, 4096, 2048], P(None, 'sp', 'tp'), may hold values from -0.09375 to 0.09375
- conv_taps: float32 [2, 31, 2048], P(None, None, 'tp'), may hold values from -9 to 9
- norm_gain: float32 [2, 2048], P(None, 'tp'), may hold values from 0.1 to 1.9
- norm_shift: float32 [2, 2048], P(None, 'tp'), may hold values from -3 to 3
- w_out: bfloat16 [2, 2048, 4096], P(None, 'tp', 'sp'), may hold values from -0.125 to 0.125
Outputs:
- hidden_out: bfloat16 [3072, 4096], P(('grp', 'sp'), 'tp'), parts along dimension 0
There are 2 independent parts, one for each index of `grp`. A program takes and returns all parts, laid end to end along the dimension named above; an argument that names none is the same for every part. Nothing has to cross between parts.
All inputs are finite; a program needn't handle non-finite values.
Results may differ from a plain program's by a relative error of at most 0.013.
Values may be sent and summed in bfloat16 or wider, within the bound.
A program may use at most 64 MiB of HBM per device.

v0:
```python
import jax
import jax.numpy as jnp
from jax import lax
from jax.sharding import PartitionSpec as P

D = 4096
C = 2048


epsilon = 1e-06


def passed_along(value, axis, steps):
    count = lax.axis_size(axis)
    initial, last = (max(0, -steps), min(count, count - steps))
    return lax.ppermute(value, axis, [(source, source + steps) for source in range(initial, last)])


def depthwise(extended, kernel_taps):
    conved = lax.conv_general_dilated(
        extended.astype(jnp.float32)[None],
        kernel_taps[:, None, :],
        (1,),
        [(0, 0)],
        dimension_numbers=("NWC", "WIO", "NWC"),
        feature_group_count=extended.shape[1],
        precision=lax.Precision.HIGHEST,
    )
    return conved[0]


def shards(hidden_in, in_gain, w_value, w_gate, conv_taps, norm_gain, norm_shift, w_out):
    layer_count = w_value.shape[0]
    reach_rows = conv_taps.shape[1] - 1
    value_all, gate_all = (
        lax.all_gather(w_value, "sp", axis=1, tiled=True),
        lax.all_gather(w_gate, "sp", axis=1, tiled=True),
    )
    out_all = lax.all_gather(w_out, "sp", axis=2, tiled=True)
    current = hidden_in
    for layer_idx in range(layer_count):
        widened = current.astype(jnp.float32)
        squares = lax.psum(jnp.sum(widened * widened, axis=1), "tp")
        normalized = (
            widened * lax.rsqrt(squares / D + epsilon)[:, None] * in_gain[layer_idx]
        ).astype(jnp.bfloat16)
        gathered = lax.all_gather(normalized, "tp", axis=1, tiled=True)
        value_part = jnp.dot(gathered, value_all[layer_idx], preferred_element_type=jnp.float32)
        gate_part = jnp.dot(gathered, gate_all[layer_idx], preferred_element_type=jnp.float32)
        gated = (value_part * jax.nn.sigmoid(gate_part)).astype(jnp.bfloat16)
        before = passed_along(gated[gated.shape[0] - reach_rows :], "sp", 1)
        extended = jnp.concatenate([before, gated], axis=0)
        residual = current
        conved = depthwise(extended, conv_taps[layer_idx])
        total_sum, total_squares = lax.psum(
            (jnp.sum(conved, axis=1), jnp.sum(conved * conved, axis=1)), "tp"
        )
        row_mean = total_sum / C
        spread = total_squares / C - row_mean * row_mean
        normed = (conved - row_mean[:, None]) * lax.rsqrt(spread + epsilon)[:, None] * norm_gain[
            layer_idx
        ] + norm_shift[layer_idx]
        mixed_out = jax.nn.silu(normed).astype(jnp.bfloat16)
        partial_value = jnp.dot(mixed_out, out_all[layer_idx], preferred_element_type=jnp.float32)
        summed = lax.psum_scatter(
            partial_value.astype(jnp.bfloat16), "tp", scatter_dimension=1, tiled=True
        ).astype(jnp.float32)
        current = (residual.astype(jnp.float32) + summed).astype(jnp.bfloat16)
    return current


def solution(mesh):
    placed = (
        P(("grp", "sp"), "tp"),
        P(None, "tp"),
        P(None, "sp", "tp"),
        P(None, "sp", "tp"),
        P(None, None, "tp"),
        P(None, "tp"),
        P(None, "tp"),
        P(None, "tp", "sp"),
    )
    return jax.shard_map(
        shards, mesh=mesh, in_specs=placed, out_specs=P(("grp", "sp"), "tp"), check_vma=False
    )
```

profile of v0, /device:TPU:24, one launch (start us, length us, event | category | flops | bytes accessed | tf_op | source)
XLA Modules:
  0.0 655.3 jit_solution(9422213232833642842)
XLA Ops:
  7.9 6.9 %psum.42 = f32[384]{0:T(512)S(1)} all-reduce(f32[384]{0:T(512)S(1)} %fusion.4), channel_id=1, replica_groups=mesh['grp'=2,'sp'=4,'tp'=4] {'tp'}, use_global_device_ids=true, to_apply=%region_1.0 | all-reduce | flops 384 | bytes 3072 | tf_op jit(solution)/shard_map/psum | solution.py:43
  15.6 2.3 fusion.6
  20.0 26.6 %all-gather.6.cloned.1.call-done = bf16[384,4096]{1,0:T(8,128)(2,1)} async-done(((bf16[384,1024]{1,0:T(8,128)(2,1)}), bf16[384,4096]{1,0:T(8,128)(2,1)}) %all-gather.6.cloned.1.call-update) | async-done | bytes 3145744 | tf_op jit(solution)/shard_map/all_gather | solution.py:47
  46.6 148.2 %all-gather.10.cloned.1.call-done = bf16[2,4096,512]{2,1,0:T(8,128)(2,1)} async-done(((bf16[2,1024,512]{2,1,0:T(8,128)(2,1)}), bf16[2,4096,512]{2,1,0:T(8,128)(2,1)}) %all-gather.10.cloned.1.call-update) | async-done | bytes 8388624 | tf_op jit(solution)/shard_map/all_gather | solution.py:37
  194.8 5.9 fusion.23
  200.7 143.5 %all-gather.8.cloned.1.call-done = bf16[2,4096,512]{2,1,0:T(8,128)(2,1)} async-done(((bf16[2,1024,512]{2,1,0:T(8,128)(2,1)}), bf16[2,4096,512]{2,1,0:T(8,128)(2,1)}) %all-gather.8.cloned.1.call-update) | async-done | bytes 8388624 | tf_op jit(solution)/shard_map/all_gather | solution.py:36
  344.2 4.2 fusion.25
  349.8 4.5 collective-permute-done
  354.8 1.9 fusion.65
  358.1 6.2 all-reduce.1
  364.3 129.2 %all-gather.12.cloned.1.call-done = bf16[2,512,4096]{2,1,0:T(8,128)(2,1)} async-done(((bf16[2,512,1024]{2,1,0:T(8,128)(2,1)}), bf16[2,512,4096]{2,1,0:T(8,128)(2,1)}) %all-gather.12.cloned.1.call-update) | async-done | bytes 8388624 | tf_op jit(solution)/shard_map/all_gather | solution.py:39
  493.4 5.9 convolution_convert_fusion.1
  499.4 39.1 %reduce-scatter.3.cloned.1.call-done = bf16[384,1024]{1,0:T(8,128)(2,1)} async-done(((bf16[384,4096]{1,0:T(8,128)(2,1)}), bf16[384,1024]{1,0:T(8,128)(2,1)}) %reduce-scatter.3.cloned.1.call-update) | async-done | bytes 786448 | tf_op jit(solution)/shard_map/reduce_scatter | solution.py:65
  539.9 5.9 psum.45
  545.9 2.3 fusion.10
  548.4 28.9 %all-gather.14.cloned.1.call-done = bf16[384,4096]{1,0:T(8,128)(2,1)} async-done(((bf16[384,1024]{1,0:T(8,128)(2,1)}), bf16[384,4096]{1,0:T(8,128)(2,1)}) %all-gather.14.cloned.1.call-update) | async-done | bytes 3145744 | tf_op jit(solution)/shard_map/all_gather | solution.py:47
  577.3 5.2 fusion.21
  582.5 4.0 fusion.24
  587.8 4.5 collective-permute-done.1
  592.8 2.0 fusion.66
  596.3 5.9 all-reduce
  602.3 5.9 convolution_convert_fusion
  608.2 37.9 %reduce-scatter.5.cloned.1.call-done = bf16[384,1024]{1,0:T(8,128)(2,1)} async-done(((bf16[384,4096]{1,0:T(8,128)(2,1)}), bf16[384,1024]{1,0:T(8,128)(2,1)}) %reduce-scatter.5.cloned.1.call-update) | async-done | bytes 786448 | tf_op jit(solution)/shard_map/reduce_scatter | solution.py:65
  646.0 2.4 fusion.11
  (64 shorter events, 12.4 us)
Async XLA Ops:
  6.5 40.0 %all-gather.6.cloned.1.call-start = ((), (), s32[]{:S(2)}) async-start(), calls=%async_computation.2 | async-start | bytes 3932160 | tf_op jit(solution)/shard_map/all_gather | solution.py:47
  17.9 2.1 copy-start.2
  17.9 176.9 %all-gather.10.cloned.1.call-start = ((), (), s32[]{:S(2)}) async-start(), calls=%async_computation.4 | async-start | bytes 10485760 | tf_op jit(solution)/shard_map/all_gather | solution.py:37
  18.6 325.5 %all-gather.8.cloned.1.call-start = ((), (), s32[]{:S(2)}) async-start(), calls=%async_computation.3 | async-start | bytes 10485760 | tf_op jit(solution)/shard_map/all_gather | solution.py:36
  19.4 474.0 %all-gather.12.cloned.1.call-start = ((), (), s32[]{:S(2)}) async-start(), calls=%async_computation.5 | async-start | bytes 10485760 | tf_op jit(solution)/shard_map/all_gather | solution.py:39
  20.0 518.5 %reduce-scatter.3.cloned.1.call-start = ((), (), s32[]{:S(2)}) async-start(), calls=%async_computation.6 | async-start | bytes 3932160 | tf_op jit(solution)/shard_map/reduce_scatter | solution.py:65
  46.6 297.6 %copy-start.4 = (bf16[384,4096]{1,0:T(8,128)(2,1)S(1)}, bf16[384,4096]{1,0:T(8,128)(2,1)}, u32[]{:S(2)}) copy-start(bf16[384,4096]{1,0:T(8,128)(2,1)} %all-gather.6.cloned.1.call-done) | copy-start | bytes 9437188
  200.7 149.1 %copy-start.3 = (f32[2,512]{1,0:T(2,128)S(1)}, f32[2,512]{1,0:T(2,128)}, u32[]{:S(2)}) copy-start(f32[2,512]{1,0:T(2,128)} %param.14) | copy-start | bytes 12292
  348.3 6.4 copy-start.6
  348.4 6.4 copy-start.7
  348.4 5.9 collective-permute-start
  499.3 39.1 %copy-start = (bf16[384,1024]{1,0:T(8,128)(2,1)S(1)}, bf16[384,1024]{1,0:T(8,128)(2,1)}, u32[]{:S(2)}) copy-start(bf16[384,1024]{1,0:T(8,128)(2,1)} %param.8) | copy-start | bytes 2359300
  499.3 78.0 %all-gather.14.cloned.1.call-start = ((), (), s32[]{:S(2)}) async-start(), calls=%async_computation.7 | async-start | bytes 3932160 | tf_op jit(solution)/shard_map/all_gather | solution.py:47
  548.2 97.8 %reduce-scatter.5.cloned.1.call-start = ((), (), s32[]{:S(2)}) async-start(), calls=%async_computation.8 | async-start | bytes 3932160 | tf_op jit(solution)/shard_map/reduce_scatter | solution.py:65
  577.3 5.2 copy-start.5
  586.5 5.8 collective-permute-start.1
  608.1 37.9 %copy-start.1 = (bf16[384,1024]{1,0:T(8,128)(2,1)S(1)}, bf16[384,1024]{1,0:T(8,128)(2,1)}, u32[]{:S(2)}) copy-start(bf16[384,1024]{1,0:T(8,128)(2,1)} %reduce-scatter.3.cloned.1.call-done) | copy-start | bytes 2359300
Sparse Core Ops, SparseCore 0:
  18.0 28.5 all-gather.5
  48.2 146.5 all-gather.9
  196.3 147.7 all-gather.7
  345.6 147.7 all-gather.11
  499.5 38.9 reduce-scatter.2
  548.3 28.9 all-gather.13
  608.3 37.7 reduce-scatter.4
where the time goes:
time: 658 us; the launch traced here: 655 us
  waiting for transfers between devices  564 us (86%)
  matrix products  35 us (5%)
  blocking collectives  25 us (4%)
  between operations  13.8 us (2%)
  other arithmetic  10.6 us (2%)
    all_gather x1, waiting for transfers between devices, shards(): lax.all_gather(w_gate, 'sp', axis=1, tiled=True)  148 us
    all_gather x1, waiting for transfers between devices, shards(): lax.all_gather(w_value, 'sp', axis=1, tiled=True)  143 us
    all_gather x1, waiting for transfers between devices, shards(): out_all = lax.all_gather(w_out, 'sp', axis=2, tiled=True)  129 us
    reduce_scatter x2, waiting for transfers between devices, shards(): lax.psum_scatter(partial_value.astype(jnp.bfloat16), 'tp', scatter_dimens...  76.9 us
    all_gather x2, waiting for transfers between devices, shards(): gathered = lax.all_gather(normalized, 'tp', axis=1, tiled=True)  55.4 us
  transfers between devices with their start and end apart: 9, of which 9 were waited for; matrix products, arithmetic and copies ran while one was open for 2% of the time, Pallas kernels for 0%

commit v1 on v0

v1 whole, which is shorter than its diff:
```python
import functools

import jax
import jax.numpy as jnp
from jax import lax
from jax.experimental import pallas as pl
from jax.experimental.pallas import tpu as pltpu
from jax.sharding import PartitionSpec as P

epsilon = 1e-06
CHUNK = 128
F32, BF16 = jnp.float32, jnp.bfloat16


def kernel(
    S, T, h_ref, gain_ref, wv_ref, wg_ref, taps_ref, ng_ref, ns_ref, wo_ref, out_ref,
    WV, WG, WO, X, ACC, EXT, CONV, MIX, PART, PRECV, SUMB, RECV, STAT, HB,
    own_sem, zr, zs_right, zs_left, yr, ys, xr, xs, xf, sr, ss, hr, hs, pr, ps, rr, rs,
):
    L = wv_ref.shape[0]
    Ds, Cn = wv_ref.shape[1], wv_ref.shape[2]
    rows, Dt = h_ref.shape
    taps = taps_ref.shape[1]
    features, channels = Dt * T, Cn * T
    chips = T // 2
    halo = EXT.shape[1] - rows
    g, me, t = lax.axis_index("grp"), lax.axis_index("sp"), lax.axis_index("tp")
    core = lax.rem(t, 2)
    chip = lax.div(t, 2)
    partner = t + 1 - 2 * core
    MESH = pl.DeviceIdType.MESH
    first, last = me == 0, me == S - 1

    sources = [(wv_ref, WV), (wg_ref, WG), (wo_ref, WO)]

    def own(layer, which):
        source, slots = sources[which]
        return pltpu.make_async_copy(source.at[layer], slots.at[layer, me], own_sem.at[layer, which])

    for layer in range(L):
        for which in range(3):
            own(layer, which).start()

    def each_chunk(body, size=CHUNK):
        def step(index, _):
            body(pl.ds(pl.multiple_of(index * size, size), size))
            return 0

        lax.fori_loop(0, rows // size, step, 0)

    def put_stat(slot, where, left, right):
        lane = lax.broadcasted_iota(jnp.int32, (left.shape[0], 128), 1)
        wide = jnp.where(lane == 0, left, right)
        STAT[slot, t, :, where] = wide.T[:8]

    def stat_copy(slot, peer):
        return pltpu.make_async_remote_copy(
            STAT.at[slot, t], STAT.at[slot, t], ss.at[slot, peer], sr.at[slot, t],
            device_id={"tp": peer}, device_id_type=MESH,
        )

    def stat_arrival(slot, peer):
        return pltpu.make_async_remote_copy(
            STAT.at[slot, peer], STAT.at[slot, peer], ss.at[slot, peer], sr.at[slot, peer],
            device_id={"tp": peer}, device_id_type=MESH,
        )

    def send_stat(slot):
        for shift in range(1, T):
            stat_copy(slot, lax.rem(t + shift, T)).start()

    def wait_stat(slot):
        for shift in range(1, T):
            stat_arrival(slot, lax.rem(t + shift, T)).wait_recv()

    def get_stat(slot, where):
        total = STAT[slot, 0, :, where]
        for peer in range(1, T):
            total = total + STAT[slot, peer, :, where]
        return jnp.concatenate([total] * 16, axis=0).T

    def half_ref(item, owner):
        kind, layer = item % 4, item // 4
        if kind < 2:
            size = Ds // 2
            return (WV, WG)[kind].at[layer, owner, pl.ds(pl.multiple_of(g * size, size), size)]
        size = Cn // 4
        start = pl.multiple_of(g * (2 * size) + (kind - 2) * size, size)
        return WO.at[layer, owner, pl.ds(start, size)]

    def other_ref(item, owner):
        kind, layer = item % 4, item // 4
        if kind < 2:
            size = Ds // 2
            return (WV, WG)[kind].at[layer, owner, pl.ds(pl.multiple_of((1 - g) * size, size), size)]
        size = Cn // 4
        start = pl.multiple_of((1 - g) * (2 * size) + (kind - 2) * size, size)
        return WO.at[layer, owner, pl.ds(start, size)]

    def zcopy(item, owner, way):
        ref = half_ref(item, owner)
        sems = zs_right if way > 0 else zs_left
        return pltpu.make_async_remote_copy(
            ref, ref, sems.at[item, owner], zr.at[item, owner],
            device_id={"sp": me + way}, device_id_type=MESH,
        )

    def ycopy(item, owner):
        ref = half_ref(item, owner)
        return pltpu.make_async_remote_copy(
            ref, ref, ys.at[item, owner], yr.at[item, owner],
            device_id={"grp": 1 - g}, device_id_type=MESH,
        )

    def yarrival(item, owner):
        ref = other_ref(item, owner)
        return pltpu.make_async_remote_copy(
            ref, ref, ys.at[item, owner], yr.at[item, owner],
            device_id={"grp": 1 - g}, device_id_type=MESH,
        )

    def event(item, k):
        if k == 0:
            if item % 4 < 3:
                own(item // 4, item % 4).wait()

            @pl.when(jnp.logical_not(last))
            def _():
                zcopy(item, me, 1).start()

            @pl.when(jnp.logical_not(first))
            def _():
                zcopy(item, me, -1).start()

            return

        @pl.when(me - k >= 0)
        def _():
            owner = me - k
            zcopy(item, owner, 1).wait_recv()

            @pl.when(jnp.logical_not(last))
            def _():
                zcopy(item, owner, 1).start()

            ycopy(item, owner).start()

        @pl.when(me + k < S)
        def _():
            owner = me + k
            zcopy(item, owner, -1).wait_recv()

            @pl.when(jnp.logical_not(first))
            def _():
                zcopy(item, owner, -1).start()

            ycopy(item, owner).start()

    def xcopy(layer, source, peer, sem):
        return pltpu.make_async_remote_copy(
            X.at[layer, source], X.at[layer, source], sem, xr.at[layer, source],
            device_id={"tp": peer}, device_id_type=MESH,
        )

    def make_x(layer):
        source = h_ref if layer == 0 else HB

        def body(where):
            wide = source[where, :].astype(F32)
            X[layer, t, where, :] = (wide * gain_ref[layer : layer + 1, :]).astype(BF16)
            squares = jnp.sum(wide * wide, axis=1, keepdims=True)
            put_stat(2 * layer, where, squares, squares)

        each_chunk(body)

    def send_x(layer):
        for shift in range(1, chips):
            peer = lax.rem(chip + shift, chips) * 2 + core
            xcopy(layer, t, peer, xs.at[layer, shift]).start()
        xcopy(layer, t, partner, xs.at[layer, 0]).start()
        send_stat(2 * layer)

    def relay_x(layer):
        for shift in range(1, chips):
            source = lax.rem(chip + shift, chips) * 2 + core
            xcopy(layer, source, partner, xf.at[layer, shift]).wait_recv()
            xcopy(layer, source, partner, xf.at[layer, shift]).start()

    def wait_x(layer):
        for shift in range(chips):
            source = lax.rem(chip + shift, chips) * 2 + 1 - core
            xcopy(layer, source, partner, xf.at[layer, 0]).wait_recv()
        wait_stat(2 * layer)

    def project(layer):
        def block(owner, _):
            @pl.when(owner != me)
            def _():
                yarrival(4 * layer, owner).wait_recv()
                yarrival(4 * layer + 1, owner).wait_recv()

            at = lax.div(owner * Ds, Dt)
            columns = pl.ds(pl.multiple_of(lax.rem(owner * Ds, Dt), 128), Ds)
            xs_block = X[layer, at, :, columns]
            for which, slots in ((0, WV), (1, WG)):
                part = jnp.dot(xs_block, slots[layer, owner], preferred_element_type=F32)

                @pl.when(owner == 0)
                def _():
                    ACC[which] = part

                @pl.when(owner > 0)
                def _():
                    ACC[which] += part

            return 0

        lax.fori_loop(0, S, block, 0)

    def halo_copy(layer):
        return pltpu.make_async_remote_copy(
            EXT.at[layer, pl.ds(rows, halo)], EXT.at[layer, pl.ds(0, halo)], hs.at[layer], hr.at[layer],
            device_id={"sp": me + 1}, device_id_type=MESH,
        )

    def gate(layer):
        def body(where):
            mean = get_stat(2 * layer, where)[:, :1] / features
            inv = lax.rsqrt(mean + epsilon)
            value, gating = ACC[0, where, :] * inv, ACC[1, where, :] * inv
            gated = (value / (1.0 + jnp.exp(-gating))).astype(BF16).astype(F32)
            EXT[layer, pl.ds(pl.multiple_of(where.start + halo, 8), where.size), :] = gated

        each_chunk(body)

        @pl.when(jnp.logical_not(last))
        def _():
            halo_copy(layer).start()

        @pl.when(first)
        def _():
            EXT[layer, pl.ds(0, halo), :] = jnp.zeros((halo, Cn), F32)

    def convolve(layer):
        @pl.when(jnp.logical_not(first))
        def _():
            halo_copy(layer).wait_recv()

        tall = CHUNK + halo + 8
        offset = halo - (taps - 1)

        def body(where):
            for column in range(0, Cn, 128):
                at = pl.ds(column, 128)
                tile = jnp.concatenate(
                    [EXT[layer, pl.ds(where.start, CHUNK + halo), at], jnp.zeros((8, 128), F32)], axis=0
                )
                total = jnp.zeros((CHUNK, 128), F32)
                for residue in range(8):
                    ks = [k for k in range(taps) if (k + offset) % 8 == residue]
                    if not ks:
                        continue
                    turned = pltpu.roll(tile, tall - residue, 0) if residue else tile
                    for k in ks:
                        low = k + offset - residue
                        total = total + taps_ref[layer, k : k + 1, at] * turned[low : low + CHUNK]
                CONV[where, at] = total
            conved = CONV[where, :]
            put_stat(
                2 * layer + 1, where,
                jnp.sum(conved, axis=1, keepdims=True),
                jnp.sum(conved * conved, axis=1, keepdims=True),
            )

        each_chunk(body)
        send_stat(2 * layer + 1)

    def mix(layer):
        wait_stat(2 * layer + 1)

        def body(where):
            stat = get_stat(2 * layer + 1, where)
            mean = stat[:, 0:1] / channels
            spread = stat[:, 1:2] / channels - mean * mean
            normed = (CONV[where, :] - mean) * lax.rsqrt(spread + epsilon) * ng_ref[
                layer : layer + 1, :
            ] + ns_ref[layer : layer + 1, :]
            MIX[where, :] = (normed / (1.0 + jnp.exp(-normed))).astype(BF16)

        each_chunk(body)

    def pair_copy(layer, at):
        return pltpu.make_async_remote_copy(
            PART.at[layer, 2 * at + 1 - core], PRECV.at[layer, at], ps.at[layer, at], pr.at[layer, at],
            device_id={"tp": partner}, device_id_type=MESH,
        )

    def sum_copy(layer, at):
        return pltpu.make_async_remote_copy(
            SUMB.at[layer, at], RECV.at[layer, chip], rs.at[layer, at], rr.at[layer, chip],
            device_id={"tp": at * 2 + core}, device_id_type=MESH,
        )

    def sum_arrival(layer, at):
        return pltpu.make_async_remote_copy(
            SUMB.at[layer, at], RECV.at[layer, at], rs.at[layer, at], rr.at[layer, at],
            device_id={"tp": at * 2 + core}, device_id_type=MESH,
        )

    def branch(layer):
        def block(owner, _):
            @pl.when(owner != me)
            def _():
                yarrival(4 * layer + 2, owner).wait_recv()
                yarrival(4 * layer + 3, owner).wait_recv()

            at = lax.div(owner * Ds, Dt)
            columns = pl.ds(pl.multiple_of(lax.rem(owner * Ds, Dt), 128), Ds)
            PART[layer, at, :, columns] = jnp.dot(
                MIX[...], WO[layer, owner], preferred_element_type=F32
            ).astype(BF16)
            return 0

        lax.fori_loop(0, S, block, 0)
        for shift in list(range(1, chips)) + [0]:
            pair_copy(layer, lax.rem(chip + shift, chips)).start()

    def reduce_pairs(layer):
        for shift in range(1, chips):
            at = lax.rem(chip + shift, chips)
            pair_copy(layer, at).wait_recv()

            def body(where, at=at):
                SUMB[layer, at, where, :] = (
                    PART[layer, at * 2 + core, where, :].astype(F32) + PRECV[layer, at, where, :].astype(F32)
                ).astype(BF16)

            each_chunk(body)
            sum_copy(layer, at).start()

    def finish(layer):
        pair_copy(layer, chip).wait_recv()
        for shift in range(1, chips):
            sum_arrival(layer, lax.rem(chip + shift, chips)).wait_recv()
        source = h_ref if layer == 0 else HB
        target = out_ref if layer == L - 1 else HB

        def body(where):
            total = PART[layer, t, where, :].astype(F32) + PRECV[layer, chip, where, :].astype(F32)
            for shift in range(1, chips):
                total = total + RECV[layer, lax.rem(chip + shift, chips), where, :].astype(F32)
            target[where, :] = (source[where, :].astype(F32) + total).astype(BF16)

        each_chunk(body)

    make_x(0)
    barrier = pltpu.get_barrier_semaphore()
    for shift in range(1, T):
        pl.semaphore_signal(barrier, inc=1, device_id={"tp": lax.rem(t + shift, T)}, device_id_type=MESH)
    pl.semaphore_signal(barrier, inc=1, device_id={"grp": 1 - g}, device_id_type=MESH)

    @pl.when(jnp.logical_not(first))
    def _():
        pl.semaphore_signal(barrier, inc=1, device_id={"sp": me - 1}, device_id_type=MESH)

    @pl.when(jnp.logical_not(last))
    def _():
        pl.semaphore_signal(barrier, inc=1, device_id={"sp": me + 1}, device_id_type=MESH)

    inner = jnp.where(first, 0, 1) + jnp.where(last, 0, 1)
    pl.semaphore_wait(barrier, T + inner)

    event(0, 0)
    event(1, 0)
    send_x(0)

    def pumped(items, stages):
        for k in range(1, S):
            for item in items:
                event(item, k)
            if stages:
                stages.pop(0)()
        for stage in stages:
            stage()

    stages = [functools.partial(relay_x, 0), functools.partial(wait_x, 0)]
    for layer in range(L):
        base = 4 * layer
        pumped([base, base + 1], stages)
        event(base + 2, 0)
        event(base + 3, 0)
        if layer + 1 < L:
            event(base + 4, 0)
        project(layer)
        gate(layer)
        pumped(
            [base + 2, base + 3],
            [functools.partial(convolve, layer), functools.partial(mix, layer)],
        )
        if layer + 1 < L:
            event(base + 5, 0)
        branch(layer)
        if layer + 1 < L:

            def next_x(layer=layer):
                finish(layer)
                make_x(layer + 1)
                send_x(layer + 1)

            def arrive_x(layer=layer):
                relay_x(layer + 1)
                wait_x(layer + 1)

            reduce_pairs(layer)
            stages = [next_x, arrive_x]
        else:
            reduce_pairs(layer)
            finish(layer)

    for item in range(4 * L):

        def drain(owner, _, item=item):
            @pl.when(jnp.logical_and(owner <= me, jnp.logical_not(last)))
            def _():
                zcopy(item, owner, 1).wait_send()

            @pl.when(jnp.logical_and(owner >= me, jnp.logical_not(first)))
            def _():
                zcopy(item, owner, -1).wait_send()

            @pl.when(owner != me)
            def _():
                ycopy(item, owner).wait_send()

            return 0

        lax.fori_loop(0, S, drain, 0)
    for layer in range(L):
        for slot in (2 * layer, 2 * layer + 1):
            for shift in range(1, T):
                stat_copy(slot, lax.rem(t + shift, T)).wait_send()
        for shift in range(chips):
            xcopy(layer, t, partner, xs.at[layer, shift]).wait_send()
            pair_copy(layer, lax.rem(chip + shift, chips)).wait_send()
        for shift in range(1, chips):
            xcopy(layer, t, partner, xf.at[layer, shift]).wait_send()
            sum_copy(layer, lax.rem(chip + shift, chips)).wait_send()

        @pl.when(jnp.logical_not(last))
        def _(layer=layer):
            halo_copy(layer).wait_send()


def shards(hidden_in, in_gain, w_value, w_gate, conv_taps, norm_gain, norm_shift, w_out):
    S, T = lax.axis_size("sp"), lax.axis_size("tp")
    L, Ds, Cn = w_value.shape
    rows, Dt = hidden_in.shape
    chips = T // 2
    halo = (conv_taps.shape[1] - 1 + 7) // 8 * 8
    vmem = pl.BlockSpec(memory_space=pltpu.VMEM)
    hbm = pl.BlockSpec(memory_space=pl.ANY)
    dma = pltpu.SemaphoreType.DMA
    return pl.pallas_call(
        functools.partial(kernel, S, T),
        out_shape=jax.ShapeDtypeStruct((rows, Dt), BF16),
        in_specs=[vmem, vmem, hbm, hbm, vmem, vmem, vmem, hbm],
        out_specs=vmem,
        scratch_shapes=[
            pltpu.VMEM((L, S, Ds, Cn), BF16),
            pltpu.VMEM((L, S, Ds, Cn), BF16),
            pltpu.VMEM((L, S, Cn, Ds), BF16),
            pltpu.VMEM((L, T, rows, Dt), BF16),
            pltpu.VMEM((2, rows, Cn), F32),
            pltpu.VMEM((L, rows + halo, Cn), F32),
            pltpu.VMEM((rows, Cn), F32),
            pltpu.VMEM((rows, Cn), BF16),
            pltpu.VMEM((L, T, rows, Dt), BF16),
            pltpu.VMEM((L, chips, rows, Dt), BF16),
            pltpu.VMEM((L, chips, rows, Dt), BF16),
            pltpu.VMEM((L, chips, rows, Dt), BF16),
            pltpu.VMEM((2 * L, T, 8, rows), F32),
            pltpu.VMEM((rows, Dt), BF16),
            dma((L, 3)),
            dma((4 * L, S)), dma((4 * L, S)), dma((4 * L, S)), dma((4 * L, S)), dma((4 * L, S)),
            dma((L, T)), dma((L, chips)), dma((L, chips)),
            dma((2 * L, T)), dma((2 * L, T)),
            dma((L,)), dma((L,)),
            dma((L, chips)), dma((L, chips)),
            dma((L, chips)), dma((L, chips)),
        ],
        compiler_params=pltpu.CompilerParams(
            collective_id=0, has_side_effects=True, vmem_limit_bytes=64_000_000
        ),
    )(hidden_in, in_gain, w_value, w_gate, conv_taps, norm_gain, norm_shift, w_out)


def solution(mesh):
    placed = (
        P(("grp", "sp"), "tp"),
        P(None, "tp"),
        P(None, "sp", "tp"),
        P(None, "sp", "tp"),
        P(None, None, "tp"),
        P(None, "tp"),
        P(None, "tp"),
        P(None, "tp", "sp"),
    )
    return jax.shard_map(
        shards, mesh=mesh, in_specs=placed, out_specs=P(("grp", "sp"), "tp"), check_vma=False
    )
```

time: 658 us -> 269 us (0.41)
  waiting for transfers between devices: 564 us -> 0 us
  Pallas kernels: 0 us -> 265 us
  matrix products: 35 us -> 0 us
  blocking collectives: 25 us -> 0 us
  between operations: 13.8 us -> 0.01 us
  other arithmetic: 10.6 us -> 0 us
    all_gather x5 -> x0, waiting for transfers between devices: 476 us -> none  [the longest x1 148 us: shards(): lax.all_gather(w_gate, 'sp', axis=1, tiled=True)]
    pallas_call x0 -> x1, Pallas kernels: none -> 265 us  [shards(): pl.pallas_call(functools.partial(kernel, S, T), out_shape=jax.ShapeDtypeS...]
    reduce_scatter x2 -> x0, waiting for transfers between devices: 76.9 us -> none  [shards(): lax.psum_scatter(partial_value.astype(jnp.bfloat16), 'tp', scatter_dimens...]
    dot_general x6 -> x0, matrix products: 31.1 us -> none  [the longest x2 11.8 us: shards(): jnp.dot(mixed_out, out_all[layer_idx], preferred_element_type=jnp.float32)]
    psum x4 -> x0, blocking collectives: 25 us -> none  [the longest x2 12.8 us: shards(): squares = lax.psum(jnp.sum(widened * widened, axis=1), 'tp')]
    ppermute x2 -> x0, waiting for transfers between devices: 8.99 us -> none  [passed_along(): lax.ppermute(value, axis, [(source, source + steps) for source in range(i...]
    convert_element_type x3 -> x0, other arithmetic: 7.03 us -> none  [the longest x2 4.59 us: shards(): normalized = (widened * lax.rsqrt(squares / D + epsilon)[:, None] * in_ga...]
  transfers between devices with their start and end apart: 9 -> 0, of which waited for: 9 -> 0; matrix products, arithmetic and copies ran while one was open for 2% -> 0% of each run, Pallas kernels for 0% -> 0%
where the time goes in v1:
time: 269 us
  Pallas kernels  265 us (99%)
  local copies, waits for them, and re-layouts  3.65 us (1%)
    pallas_call x1, Pallas kernels, shards(): pl.pallas_call(functools.partial(kernel, S, T), out_shape=jax.ShapeDtypeS...  265 us

profile of v1, /device:TPU:24, one launch (start us, length us, event | category | flops | bytes accessed | tf_op | source)
XLA Modules:
  0.0 268.6 jit_solution(2188554346435261257)
XLA Ops:
  0.0 1.6 copy.9.taps_ref
  1.6 264.9 %shard_map.82 = bf16[384,1024]{1,0:T(8,128)(2,1)} custom-call(bf16[384,1024]{1,0:T(8,128)(2,1)} %h_ref.1, f32[2,1024]{1,0:T(2,128)} %gain_ref.1, bf16[2,1024,512]{2,1,0:T(8,128)(2,1)} %wv_ref.1, bf16[2,1024,512]{2,1,0:T(8,128)(2,1)} %wg_ref.1, f32[2,31,512]{2,1,0:T(8,128)} %copy.9.taps_ref, f32[2,512]{1,0:T(2,128)} %ng_ref.1, f32[2,512]{1,0:T(2,128)} %ns_ref.1, ...), custom_call_target="tpu_custom_call" | custom-call | tf_op jit(solution)/shard_map/pallas_call | solution.py:463
  266.5 2.1 copy.11

commit v2 on v1

--- a/solution.py
+++ b/solution.py
@@ -192,9 +192,22 @@
             xcopy(layer, source, partner, xf.at[layer, 0]).wait_recv()
         wait_stat(2 * layer)
 
+    def by_arrival(body):
+        def step(turn, _):
+            away = lax.div(turn + 1, 2)
+            owner = jnp.where(lax.rem(turn, 2) == 1, me + away, me - away)
+
+            @pl.when(jnp.logical_and(owner >= 0, owner < S))
+            def _():
+                body(turn, owner)
+
+            return 0
+
+        lax.fori_loop(0, 2 * S - 1, step, 0)
+
     def project(layer):
-        def block(owner, _):
-            @pl.when(owner != me)
+        def block(turn, owner):
+            @pl.when(turn > 0)
             def _():
                 yarrival(4 * layer, owner).wait_recv()
                 yarrival(4 * layer + 1, owner).wait_recv()
@@ -205,17 +218,15 @@
             for which, slots in ((0, WV), (1, WG)):
                 part = jnp.dot(xs_block, slots[layer, owner], preferred_element_type=F32)
 
-                @pl.when(owner == 0)
+                @pl.when(turn == 0)
                 def _():
                     ACC[which] = part
 
-                @pl.when(owner > 0)
+                @pl.when(turn > 0)
                 def _():
                     ACC[which] += part
 
-            return 0
-
-        lax.fori_loop(0, S, block, 0)
+        by_arrival(block)
 
     def halo_copy(layer):
         return pltpu.make_async_remote_copy(
@@ -307,36 +318,46 @@
             device_id={"tp": at * 2 + core}, device_id_type=MESH,
         )
 
+    def sum_pair(layer, at):
+        pair_copy(layer, at).wait_recv()
+
+        def body(where):
+            SUMB[layer, at, where, :] = (
+                PART[layer, at * 2 + core, where, :].astype(F32) + PRECV[layer, at, where, :].astype(F32)
+            ).astype(BF16)
+
+        each_chunk(body)
+        sum_copy(layer, at).start()
+
     def branch(layer):
-        def block(owner, _):
-            @pl.when(owner != me)
+        def block(turn, owner):
+            @pl.when(turn > 0)
             def _():
                 yarrival(4 * layer + 2, owner).wait_recv()
                 yarrival(4 * layer + 3, owner).wait_recv()
 
-            at = lax.div(owner * Ds, Dt)
+            target = lax.div(owner * Ds, Dt)
             columns = pl.ds(pl.multiple_of(lax.rem(owner * Ds, Dt), 128), Ds)
-            PART[layer, at, :, columns] = jnp.dot(
+            PART[layer, target, :, columns] = jnp.dot(
                 MIX[...], WO[layer, owner], preferred_element_type=F32
             ).astype(BF16)
-            return 0
-
-        lax.fori_loop(0, S, block, 0)
-        for shift in list(range(1, chips)) + [0]:
-            pair_copy(layer, lax.rem(chip + shift, chips)).start()
-
-    def reduce_pairs(layer):
-        for shift in range(1, chips):
-            at = lax.rem(chip + shift, chips)
-            pair_copy(layer, at).wait_recv()
-
-            def body(where, at=at):
-                SUMB[layer, at, where, :] = (
-                    PART[layer, at * 2 + core, where, :].astype(F32) + PRECV[layer, at, where, :].astype(F32)
-                ).astype(BF16)
-
-            each_chunk(body)
-            sum_copy(layer, at).start()
+            if S == T:
+                at = lax.div(target, 2)
+
+                @pl.when(lax.rem(target, 2) != core)
+                def _():
+                    pair_copy(layer, at).start()
+
+                @pl.when(jnp.logical_and(lax.rem(target, 2) == core, at != chip))
+                def _():
+                    sum_pair(layer, at)
+
+        by_arrival(block)
+        if S != T:
+            for shift in list(range(1, chips)) + [0]:
+                pair_copy(layer, lax.rem(chip + shift, chips)).start()
+            for shift in range(1, chips):
+                sum_pair(layer, lax.rem(chip + shift, chips))
 
     def finish(layer):
         pair_copy(layer, chip).wait_recv()
@@ -353,7 +374,6 @@
 
         each_chunk(body)
 
-    make_x(0)
     barrier = pltpu.get_barrier_semaphore()
     for shift in range(1, T):
         pl.semaphore_signal(barrier, inc=1, device_id={"tp": lax.rem(t + shift, T)}, device_id_type=MESH)
@@ -372,10 +392,11 @@
 
     event(0, 0)
     event(1, 0)
+    make_x(0)
     send_x(0)
 
-    def pumped(items, stages):
-        for k in range(1, S):
+    def pumped(items, stages, start=1):
+        for k in range(start, S):
             for item in items:
                 event(item, k)
             if stages:
@@ -384,11 +405,16 @@
             stage()
 
     stages = [functools.partial(relay_x, 0), functools.partial(wait_x, 0)]
+    ahead = 1
     for layer in range(L):
         base = 4 * layer
-        pumped([base, base + 1], stages)
+        if ahead > 1:
+            event(base + 1, 1)
+        pumped([base, base + 1], stages, ahead)
         event(base + 2, 0)
         event(base + 3, 0)
+        event(base + 2, 1)
+        event(base + 3, 1)
         if layer + 1 < L:
             event(base + 4, 0)
         project(layer)
@@ -396,9 +422,12 @@
         pumped(
             [base + 2, base + 3],
             [functools.partial(convolve, layer), functools.partial(mix, layer)],
+            2,
         )
         if layer + 1 < L:
             event(base + 5, 0)
+            event(base + 4, 1)
+            ahead = 2
         branch(layer)
         if layer + 1 < L:
 
@@ -411,10 +440,8 @@
                 relay_x(layer + 1)
                 wait_x(layer + 1)
 
-            reduce_pairs(layer)
             stages = [next_x, arrive_x]
         else:
-            reduce_pairs(layer)
             finish(layer)
 
     for item in range(4 * L):

time: 269 us -> 247 us (0.918)
  Pallas kernels: 265 us -> 243 us
    pallas_call x1, Pallas kernels: 265 us -> 243 us  [shards(): pl.pallas_call(functools.partial(kernel, S, T), out_shape=jax.ShapeDtypeS...]
where the time goes in v2:
time: 247 us
  Pallas kernels  243 us (98%)
  local copies, waits for them, and re-layouts  3.65 us (1%)
    pallas_call x1, Pallas kernels, shards(): pl.pallas_call(functools.partial(kernel, S, T), out_shape=jax.ShapeDtypeS...  243 us

profile of v2, /device:TPU:24, one launch (start us, length us, event | category | flops | bytes accessed | tf_op | source)
XLA Modules:
  0.0 246.7 jit_solution(10247928322247583299)
XLA Ops:
  0.0 1.6 copy.9.taps_ref
  1.6 243.0 %shard_map.82 = bf16[384,1024]{1,0:T(8,128)(2,1)} custom-call(bf16[384,1024]{1,0:T(8,128)(2,1)} %h_ref.1, f32[2,1024]{1,0:T(2,128)} %gain_ref.1, bf16[2,1024,512]{2,1,0:T(8,128)(2,1)} %wv_ref.1, bf16[2,1024,512]{2,1,0:T(8,128)(2,1)} %wg_ref.1, f32[2,31,512]{2,1,0:T(8,128)} %copy.9.taps_ref, f32[2,512]{1,0:T(2,128)} %ng_ref.1, f32[2,512]{1,0:T(2,128)} %ns_ref.1, ...), custom_call_target="tpu_custom_call" | custom-call | tf_op jit(solution)/shard_map/pallas_call | solution.py:490
  244.6 2.1 copy.11
